TPU v7x, 256 devices: a whole 4x4x8 slice. The times are simulated.
256 devices in a mesh: sp: 64 (over z, x, core), tp: 4 (over y).
Axes of the slice: x: 4, y: 4, z: 8, core: 2. Of those that a mesh axis runs over, the one named last changes fastest.
Arguments:
- cot_out: bfloat16 [16384, 2048], P('sp', 'tp'), may hold values from -16 to 16
- route_ids: int32 [16384, 2], P('sp'), may hold values from 0 to 63, all different within a row; in each aligned block of 256 rows (0 to 255, 256 to 511, ...) at most 12 rows name the same one
- route_weight: float32 [16384, 2], P('sp'), may hold values from 0.1 to 1
- expert_inputs: bfloat16 [64, 768, 2048], P('sp'), may hold values from -48 to 48
- w_gate: bfloat16 [64, 2048, 1024], P('sp', None, 'tp'), may hold values from -0.125 to 0.125
- w_up: bfloat16 [64, 2048, 1024], P('sp', None, 'tp'), may hold values from -0.125 to 0.125
- w_down: bfloat16 [64, 1024, 2048], P('sp', 'tp'), may hold values from -0.1875 to 0.1875
- w_proj: bfloat16 [2048, 2048], P('tp'), may hold values from -0.125 to 0.125
- conv_out: bfloat16 [16384, 2048], P('sp', 'tp'), may hold values from -6 to 6
- channel_norm_gain: float32 [2048], P('tp'), may hold values from 0.1 to 1.9
- taps: float32 [31, 2048], P(None, 'tp'), may hold values from -1 to 1
- value_pre: bfloat16 [16384, 2048], P('sp', 'tp'), may hold values from -6 to 6
- gate_pre: bfloat16 [16384, 2048], P('sp', 'tp'), may hold values from -6 to 6
Outputs:
- grad_gate_w: bfloat16 [64, 2048, 1024], P('sp', None, 'tp')
- grad_up_w: bfloat16 [64, 2048, 1024], P('sp', None, 'tp')
- grad_down_w: bfloat16 [64, 1024, 2048], P('sp', 'tp')
- grad_proj: float32 [2048, 2048], P(('tp', 'sp'))
- grad_value: bfloat16 [16384, 2048], P('sp', 'tp')
- grad_gate: bfloat16 [16384, 2048], P('sp', 'tp')
Inputs may be any that keep to these rules, and one draw needn't show every extreme that they name: `route_ids`: among the tokens of one index of sp no expert is chosen more than 12 times, a bound that some block reaches; a token's experts differ.
All inputs are finite; a program needn't handle non-finite values.
Results may differ from a plain program's by a relative error of at most 0.012.
Values may be sent and summed in bfloat16 or wider, within the bound.
No kernel may reach another device: no remote copies, remote signals or barrier semaphores. Data moves between devices by JAX's collectives and lax.ppermute only.
A program may use at most 128 MiB of HBM per device.

v0:
```python
import jax
import jax.numpy as jnp
from jax import lax
from jax.sharding import Mesh
from jax.sharding import PartitionSpec as P

SP = ("sp_0", "sp_1", "sp_2")
TP_SP = ("tp", "sp_0", "sp_1", "sp_2")
clamp_limit = 7.0
swish_alpha = 1.702
norm_epsilon = 1e-05


def in_blocks(value, dim, devices):
    dims = value.shape
    tiles = value.reshape(*dims[:dim], devices, dims[dim] // devices, *dims[dim + 1 :])
    return jnp.moveaxis(tiles, dim, 0)


def sum_at_owner(value, axis, dim):
    tiles = in_blocks(value, dim, lax.axis_size(axis))
    arrived = lax.all_to_all(tiles, axis, split_axis=0, concat_axis=0, tiled=True)
    return arrived.astype(jnp.float32).sum(axis=0)


def from_everyone(value, axis):
    devices = lax.axis_size(axis)
    return lax.all_to_all(
        jnp.broadcast_to(value[None], (devices, *value.shape)), axis, 0, 0, tiled=True
    )


def in_order(tiles, dim):
    dims = list(tiles.shape[1:])
    dims[dim] *= tiles.shape[0]
    return jnp.moveaxis(tiles, 0, dim).reshape(dims)


def collect(value, axis, dim):
    tiles = from_everyone(value, axis)
    return in_order(tiles, dim)


def sum_by_axis(subtotal, axes):
    for axis in axes:
        subtotal = lax.psum_scatter(subtotal, axis, scatter_dimension=0, tiled=True)
    return subtotal


def of_everyone(value, axis):
    return from_everyone(value, axis).sum(axis=0)


def in_one(arrays, axis):
    flat, at, done = (jnp.concatenate([a.reshape(-1) for a in arrays]), 0, [])
    subtotal = of_everyone(flat, axis)
    for a in arrays:
        done.append(subtotal[at : at + a.size].reshape(a.shape))
        at += a.size
    return tuple(done)


def passed_along(value, axis, steps):
    count = lax.axis_size(axis)
    leading, last = (max(0, -steps), min(count, count - steps))
    return lax.ppermute(value, axis, [(source, source + steps) for source in range(leading, last)])


def per_device(
    cot_out,
    route_ids,
    route_weight,
    expert_inputs,
    w_gate,
    w_up,
    w_down,
    w_proj,
    conv_out,
    channel_norm_gain,
    taps,
    value_pre,
    gate_pre,
):
    group_size = lax.axis_size(SP)
    narrow_size = lax.axis_size("tp")
    tok_rows = cot_out.shape[0]
    chosen = route_ids.shape[1]
    slot_rows = expert_inputs.shape[1]
    capacity = slot_rows // group_size
    model_width = expert_inputs.shape[2]
    local_cols = cot_out.shape[1]
    flat_ids = route_ids.reshape(-1)
    expert_hot = (flat_ids[:, None] == jnp.arange(group_size, dtype=jnp.int32)[None, :]).astype(
        jnp.int32
    )
    earlier = jnp.sum((jnp.cumsum(expert_hot, axis=0) - expert_hot) * expert_hot, axis=1)
    dest_rows = flat_ids * capacity + earlier
    flat_weight = route_weight.reshape(-1)[:, None]
    scaled = (flat_weight * jnp.repeat(cot_out, chosen, axis=0).astype(jnp.float32)).astype(
        jnp.bfloat16
    )
    outgoing = (
        jnp.zeros((group_size * capacity, local_cols), jnp.bfloat16).at[dest_rows].set(scaled)
    )
    moved = lax.all_to_all(
        outgoing.reshape(group_size, capacity, local_cols),
        SP,
        split_axis=0,
        concat_axis=0,
        tiled=True,
    )
    arrived = lax.all_gather(moved, "tp", axis=2, tiled=True)
    rows_cot = arrived.reshape(slot_rows, model_width)
    rows_in = expert_inputs[0]
    gate_weight = w_gate[0]
    up_weight = w_up[0]
    down_weight = w_down[0]
    gate_lin = jnp.dot(rows_in, gate_weight, preferred_element_type=jnp.float32)
    up_lin = jnp.dot(rows_in, up_weight, preferred_element_type=jnp.float32)
    gate_c = jnp.minimum(gate_lin, clamp_limit)
    up_c = jnp.clip(up_lin, -clamp_limit, clamp_limit)
    sigma = jax.nn.sigmoid(swish_alpha * gate_c)
    act = ((up_c + 1.0) * gate_c * sigma).astype(jnp.bfloat16)
    grad_down = jnp.dot(act.T, rows_cot, preferred_element_type=jnp.float32).astype(jnp.bfloat16)
    d_act = jnp.dot(rows_cot, down_weight.T, preferred_element_type=jnp.float32)
    up_open = ((up_lin > -clamp_limit) & (up_lin < clamp_limit)).astype(jnp.float32)
    gate_open = (gate_lin < clamp_limit).astype(jnp.float32)
    d_up = (d_act * gate_c * sigma * up_open).astype(jnp.bfloat16)
    d_gate = (
        d_act * (up_c + 1.0) * (sigma + swish_alpha * gate_c * sigma * (1.0 - sigma)) * gate_open
    ).astype(jnp.bfloat16)
    grad_gate_part = jnp.dot(rows_in.T, d_gate, preferred_element_type=jnp.float32).astype(
        jnp.bfloat16
    )
    grad_up_part = jnp.dot(rows_in.T, d_up, preferred_element_type=jnp.float32).astype(jnp.bfloat16)
    partial_value = jnp.dot(d_gate, gate_weight.T, preferred_element_type=jnp.float32)
    partial_value = partial_value + jnp.dot(d_up, up_weight.T, preferred_element_type=jnp.float32)
    input_grad = sum_at_owner(partial_value.astype(jnp.bfloat16), "tp", 1).astype(jnp.bfloat16)
    coming = lax.all_to_all(
        input_grad.reshape(group_size, capacity, local_cols),
        SP,
        split_axis=0,
        concat_axis=0,
        tiled=True,
    )
    picked = coming.reshape(group_size * capacity, local_cols)[dest_rows].astype(jnp.float32)
    summed = jnp.sum(picked.reshape(tok_rows, chosen, local_cols), axis=1)
    mix_grad = (cot_out.astype(jnp.float32) + summed).astype(jnp.bfloat16)
    mix_full = collect(mix_grad, "tp", 1)
    convolution_filter = conv_out.astype(jnp.float32)
    channel_total = local_cols * narrow_size
    first_sum, square_sum = lax.psum(
        (
            jnp.sum(convolution_filter, axis=1),
            jnp.sum(convolution_filter * convolution_filter, axis=1),
        ),
        "tp",
    )
    channel_mean = (first_sum / channel_total)[:, None]
    var = (square_sum / channel_total)[:, None] - channel_mean * channel_mean
    inverse_deviation = lax.rsqrt(var + norm_epsilon)
    normalized_input = (convolution_filter - channel_mean) * inverse_deviation
    normalized_output = normalized_input * channel_norm_gain[None, :]
    sigma_conv = jax.nn.sigmoid(normalized_output)
    act_conv = (normalized_output * sigma_conv).astype(jnp.bfloat16)
    grad_proj = sum_by_axis(
        lax.dot_general(
            act_conv, mix_full, (((0,), (0,)), ((), ())), preferred_element_type=jnp.float32
        ),
        SP,
    )
    d_act_conv = jnp.dot(mix_full, w_proj.T, preferred_element_type=jnp.float32)
    normalized_gradient = (
        d_act_conv
        * sigma_conv
        * (1.0 + normalized_output * (1.0 - sigma_conv))
        * channel_norm_gain[None, :]
    )
    first_term_gradient, second_term_gradient = in_one(
        (
            jnp.sum(normalized_gradient, axis=1),
            jnp.sum(normalized_gradient * normalized_input, axis=1),
        ),
        "tp",
    )
    convolution_gradient = inverse_deviation * (
        normalized_gradient
        - (first_term_gradient / channel_total)[:, None]
        - normalized_input * (second_term_gradient / channel_total)[:, None]
    )
    reach = taps.shape[0]
    following = passed_along(convolution_gradient[: reach - 1], SP, -1)
    extended = jnp.concatenate([convolution_gradient, following], axis=0)
    d_glu = jnp.zeros_like(convolution_gradient)
    for offset in range(reach):
        begin = reach - 1 - offset
        d_glu = d_glu + taps[offset][None, :] * extended[begin : begin + tok_rows]
    gate_sig = jax.nn.sigmoid(gate_pre.astype(jnp.float32))
    grad_value = (d_glu * gate_sig).astype(jnp.bfloat16)
    grad_gate = (d_glu * value_pre.astype(jnp.float32) * gate_sig * (1.0 - gate_sig)).astype(
        jnp.bfloat16
    )
    return (
        grad_gate_part[None],
        grad_up_part[None],
        grad_down[None],
        grad_proj,
        grad_value,
        grad_gate,
    )


def solution(mesh):
    finer = Mesh(mesh.devices.reshape(8, 4, 2, mesh.shape["tp"]), ("sp_0", "sp_1", "sp_2", "tp"))
    placed = (
        P(SP, "tp"),
        P(SP, None),
        P(SP, None),
        P(SP, None, None),
        P(SP, None, "tp"),
        P(SP, None, "tp"),
        P(SP, "tp", None),
        P("tp", None),
        P(SP, "tp"),
        P("tp"),
        P(None, "tp"),
        P(SP, "tp"),
        P(SP, "tp"),
    )
    return jax.shard_map(
        per_device,
        mesh=finer,
        in_specs=placed,
        out_specs=(
            P(SP, None, "tp"),
            P(SP, None, "tp"),
            P(SP, "tp", None),
            P(TP_SP, None),
            P(SP, "tp"),
            P(SP, "tp"),
        ),
        check_vma=False,
    )
```

profile of v0, /device:TPU:1, one launch (start us, length us, event | category | flops | bytes accessed | tf_op | source)
XLA Modules:
  0.0 352.8 jit_solution(16087362731274032509)
XLA Ops:
  7.2 0.0 all-gather.2.cloned.1.call-start
  7.2 0.8 broadcast_multiply_fusion
  8.1 0.9 copy.48
  9.0 0.1 eq.25
  9.1 0.1 eq.29
  9.3 0.1 copy.47
  9.4 0.1 mul.445
  9.6 1.2 reduce-window.6
  10.8 0.2 slice_reduce_fusion
  11.0 2.2 broadcast_in_dim.15
  13.2 2.9 convert_element_type.80
  16.2 0.1 copy.51
  16.3 0.1 mul.447
  16.4 0.1 fusion.150
  16.6 4.1 %scatter_custom_fusion = bf16[768,512]{1,0:T(8,128)(2,1)} fusion(s32[512]{0:T(512)S(1)} %bitcast.147, f32[512,512]{1,0:T(8,128)} %convert_element_type.80, f32[512]{0:T(512)S(1)} %mul.447, bf16[]{:T(256)} %constant.12.clone.1), kind=kCustom, calls=%fused_computation.199 | custom fusion | flops 524288 | bytes 1837058 | tf_op jit(solution)/shard_map/scatter | solution.py:103
  20.6 2.1 reshape.100
  22.7 41.2 %all_to_all.26 = bf16[64,12,512]{2,1,0:T(8,128)(2,1)} all-to-all(bf16[64,12,512]{2,1,0:T(8,128)(2,1)} %reshape.100), channel_id=1, replica_groups=mesh['sp_0'=8,'sp_1'=4,'sp_2'=2,'tp'=4] {'sp_0','sp_1','sp_2'}, dimensions={0} | all-to-all | bytes 1572864 | tf_op jit(solution)/shard_map/all_to_all | solution.py:105
  64.0 3.2 fusion.4
  67.2 1.9 fusion.6
  69.1 42.8 %all-gather.2.cloned.1.call-done = bf16[64,12,2048]{2,1,0:T(8,128)(2,1)} async-done(((bf16[64,12,512]{2,1,0:T(8,128)(2,1)}), bf16[64,12,2048]{2,1,0:T(8,128)(2,1)}) %all-gather.2.cloned.1.call-update) | async-done | bytes 3145744 | tf_op jit(solution)/shard_map/all_gather | solution.py:112
  111.9 6.2 %reshape.101 = bf16[768,2048]{1,0:T(8,128)(2,1)} reshape(bf16[64,12,2048]{2,1,0:T(8,128)(2,1)} %all-gather.2.cloned.1.call-done) | data formatting | bytes 6291456 | tf_op jit(solution)/shard_map/reshape | solution.py:113
  118.0 4.1 %select_convert_fusion = (bf16[768,256]{1,0:T(8,128)(2,1)S(1)}, bf16[768,256]{1,0:T(8,128)(2,1)S(1)}) fusion(f32[768,256]{1,0:T(8,128)} %fusion.4, f32[768,256]{1,0:T(8,128)} %fusion.6, bf16[768,2048]{1,0:T(8,128)(2,1)} %reshape.101, bf16[1,256,2048]{2,1,0:T(8,128)(2,1)} %param.19), kind=kOutput, calls=%fused_computation.62 | convolution fusion | flops 809828352 | bytes 6553600 | tf_op jit(solution)/shard_map/dot_general | solution.py:125
  122.2 1.0 fusion.27
  123.2 0.4 copy-done.7
  123.7 1.0 add_convert_fusion
  124.7 0.2 copy.64
  125.0 39.9 %all_to_all.27 = bf16[4,768,512]{2,1,0:T(8,128)(2,1)} all-to-all(bf16[4,768,512]{2,1,0:T(8,128)(2,1)S(1)} %bitcast.113), channel_id=1, replica_groups=mesh['sp_0'=8,'sp_1'=4,'sp_2'=2,'tp'=4] {'tp'}, dimensions={0} | all-to-all | bytes 6291456 | tf_op jit(solution)/shard_map/all_to_all | solution.py:22
  164.9 3.5 reduce_sum.81
  168.4 2.1 reshape.103
  170.5 12.1 %all-to-all-start.2 = ((bf16[64,12,512]{2,1,0:T(8,128)(2,1)}), bf16[64,12,512]{2,1,0:T(8,128)(2,1)}, u32[]{:S(2)}, u32[]{:S(2)}) async-start(bf16[64,12,512]{2,1,0:T(8,128)(2,1)} %reshape.103), calls=%async_computation.2 | async-start | bytes 2097152 | tf_op jit(solution)/shard_map/all_to_all | solution.py:139
  182.6 28.1 %all-to-all-done.2 = bf16[64,12,512]{2,1,0:T(8,128)(2,1)} async-done(((bf16[64,12,512]{2,1,0:T(8,128)(2,1)}), bf16[64,12,512]{2,1,0:T(8,128)(2,1)}, u32[]{:S(2)}, u32[]{:S(2)}) %all-to-all-start.2) | async-done | bytes 786464 | tf_op jit(solution)/shard_map/all_to_all | solution.py:139
  210.6 2.1 reshape.104
  212.7 3.9 %gather_fusion = bf16[512,512]{1,0:T(8,128)(2,1)} fusion(bf16[768,512]{1,0:T(8,128)(2,1)} %reshape.104, s32[1024]{0:T(1024)S(1)} %pad_clamp_fusion), kind=kCustom, calls=%fused_computation | custom fusion | bytes 1050624 | tf_op jit(solution)/shard_map/gather | solution.py:146
  216.6 2.7 reshape.106
  219.2 3.3 reduce_sum.82
  222.5 1.9 add_convert_fusion.1
  224.4 1.8 copy.53
  226.2 2.0 broadcast_in_dim.19
  228.2 4.2 %all-to-all-start.3 = ((bf16[4,256,512]{1,2,0:T(8,128)(2,1)}), bf16[4,256,512]{1,2,0:T(8,128)(2,1)}, u32[]{:S(2)}, u32[]{:S(2)}) async-start(bf16[4,256,512]{1,2,0:T(8,128)(2,1)} %broadcast_in_dim.19), calls=%async_computation.3 | async-start | bytes 2097152 | tf_op jit(solution)/shard_map/all_to_all | solution.py:28
  232.4 0.0 reduce-scatter.4.cloned.1.call-start
  232.5 0.2 convert_reduce_fusion
  232.7 15.6 %all-reduce = (f32[256]{0:T(256)S(1)}, f32[256]{0:T(256)S(1)}) all-reduce(f32[256]{0:T(256)S(1)} %get-tuple-element.39, f32[256]{0:T(256)S(1)} %get-tuple-element.38), channel_id=1, replica_groups=mesh['sp_0'=8,'sp_1'=4,'sp_2'=2,'tp'=4] {'tp'}, use_global_device_ids=true, to_apply=%region_7.8 | all-reduce | flops 512 | bytes 4096 | tf_op jit(solution)/shard_map/psum | solution.py:152
  248.3 4.1 %fusion.142 = f32[512,2048]{1,0:T(8,128)} fusion(bf16[256,2048]{0,1:T(8,128)(2,1)} %bitcast.14, bf16[256,512]{1,0:T(8,128)(2,1)S(1)} %copy-done.2, f32[512]{0:T(512)S(1)} %copy-done.11, f32[256]{0:T(256)S(1)} %get-tuple-element.80, f32[256]{0:T(256)S(1)} %get-tuple-element.79), kind=kOutput, calls=%fused_computation.212 | convolution fusion | flops 538050560 | bytes 5509120 | tf_op jit(solution)/shard_map/dot_general | solution.py:167
  252.4 0.8 copy-done.9
  253.2 0.6 fusion.160
  253.8 0.7 fusion.159
  254.5 4.6 %fusion.14 = bf16[1,256,2048]{2,1,0:T(8,128)(2,1)} fusion(bf16[768,2048]{1,0:T(8,128)(2,1)} %reshape.101, f32[768,256]{1,0:T(8,128)} %fusion.6, f32[768,256]{1,0:T(8,128)} %fusion.4), kind=kOutput, calls=%fused_computation.44 | convolution fusion | flops 807796736 | bytes 5767168 | tf_op jit(solution)/shard_map/dot_general | solution.py:124
  259.1 3.0 fusion.157
  262.1 0.6 broadcast_in_dim.20
  262.7 3.2 all-to-all-start.4
  266.0 0.0 reduce-scatter.6.cloned.1.call-start
  266.0 38.5 %reduce-scatter.4.cloned.1.call-done = f32[64,2048]{1,0:T(8,128)} async-done(((f32[512,2048]{1,0:T(8,128)}), f32[64,2048]{1,0:T(8,128)}) %reduce-scatter.4.cloned.1.call-update) | async-done | bytes 524304 | tf_op jit(solution)/shard_map/reduce_scatter | solution.py:46
  304.5 0.0 reduce-scatter.8.cloned.1.call-start
  304.5 3.0 fusion.18
  307.6 1.2 fusion.132
  308.8 0.8 copy-done.1
  309.6 2.9 collective-permute-start
  312.5 3.0 fusion.15
  315.5 2.3 copy.55
  317.8 2.3 copy.56
  320.0 7.5 %reduce-scatter.6.cloned.1.call-done = f32[16,2048]{1,0:T(8,128)} async-done(((f32[64,2048]{1,0:T(8,128)}), f32[16,2048]{1,0:T(8,128)}) %reduce-scatter.6.cloned.1.call-update) | async-done | bytes 131088 | tf_op jit(solution)/shard_map/reduce_scatter | solution.py:46
  327.6 11.4 %multiply_convert_fusion.3 = (bf16[256,512]{1,0:T(8,128)(2,1)}, f32[256,512]{1,0:T(8,128)S(1)}) fusion(bf16[256,512]{1,0:T(8,128)(2,1)} %param.24, bf16[256,512]{1,0:T(8,128)(2,1)S(1)} %copy-done.6, f32[256,512]{1,0:T(8,128)} %copy-done.1, f32[512]{0:T(512)} %bitcast.125, f32[30,512]{1,0:T(8,128)S(1)} %collective-permute-done, f32[512]{0:T(512)} %bitcast.126, ...), kind=kLoop, calls=%fused_computation.202 | loop fusion | flops 13238272 | bytes 1959936 | tf_op jit(solution)/shard_map/convert_element_type | solution.py:200
  339.0 0.9 multiply_convert_fusion.4
  339.8 6.4 %reduce-scatter.8.cloned.1.call-done = f32[8,2048]{1,0:T(8,128)} async-done(((f32[16,2048]{1,0:T(8,128)}), f32[8,2048]{1,0:T(8,128)}) %reduce-scatter.8.cloned.1.call-update) | async-done | bytes 65552 | tf_op jit(solution)/shard_map/reduce_scatter | solution.py:46
  (40 shorter events, 0.3 us)
Async XLA Ops:
  7.2 56.8 %copy-start = (bf16[1,768,2048]{2,1,0:T(8,128)(2,1)S(1)}, bf16[1,768,2048]{2,1,0:T(8,128)(2,1)}, u32[]{:S(2)}) copy-start(bf16[1,768,2048]{2,1,0:T(8,128)(2,1)} %param.16) | copy-start | bytes 9437188
  7.2 9.0 %copy-start.10 = (f32[256,2]{0,1:T(2,128)S(1)}, f32[256,2]{0,1:T(2,128)}, u32[]{:S(2)}) copy-start(f32[256,2]{0,1:T(2,128)} %param.15) | copy-start | bytes 6148
  7.2 104.7 %all-gather.2.cloned.1.call-start = ((), (), s32[]{:S(2)}) async-start(), calls=%async_computation.8 | async-start | bytes 5242880 | tf_op jit(solution)/shard_map/all_gather | solution.py:112
  64.0 3.2 copy-start.4
  118.0 4.2 %copy-start.5 = (bf16[1,2048,256]{2,1,0:T(8,128)(2,1)S(1)}, bf16[1,2048,256]{2,1,0:T(8,128)(2,1)}, u32[]{:S(2)}) copy-start(bf16[1,2048,256]{2,1,0:T(8,128)(2,1)} %param.17) | copy-start | bytes 3145732
  122.2 1.1 copy-start.3
  122.2 1.1 copy-start.8
  122.2 1.5 copy-start.7
  170.5 40.2 %all-to-all-start.2 = ((bf16[64,12,512]{2,1,0:T(8,128)(2,1)}), bf16[64,12,512]{2,1,0:T(8,128)(2,1)}, u32[]{:S(2)}, u32[]{:S(2)}) async-start(bf16[64,12,512]{2,1,0:T(8,128)(2,1)} %reshape.103), calls=%async_computation.2 | async-start | bytes 2097152 | tf_op jit(solution)/shard_map/all_to_all | solution.py:139
  219.2 13.3 %copy-start.2 = (bf16[256,512]{1,0:T(8,128)(2,1)S(1)}, bf16[256,512]{1,0:T(8,128)(2,1)}, u32[]{:S(2)}) copy-start(bf16[256,512]{1,0:T(8,128)(2,1)} %param.21) | copy-start | bytes 786436
  219.2 29.0 %copy-start.11 = (f32[512]{0:T(512)S(1)}, f32[512]{0:T(512)}, u32[]{:S(2)}) copy-start(f32[512]{0:T(512)} %param.22) | copy-start | bytes 6148
  228.2 20.1 %all-to-all-start.3 = ((bf16[4,256,512]{1,2,0:T(8,128)(2,1)}), bf16[4,256,512]{1,2,0:T(8,128)(2,1)}, u32[]{:S(2)}, u32[]{:S(2)}) async-start(bf16[4,256,512]{1,2,0:T(8,128)(2,1)} %broadcast_in_dim.19), calls=%async_computation.3 | async-start | bytes 2097152 | tf_op jit(solution)/shard_map/all_to_all | solution.py:28
  232.4 72.0 %reduce-scatter.4.cloned.1.call-start = ((), (), s32[]{:S(2)}) async-start(), calls=%async_computation.9 | async-start | bytes 4718592 | tf_op jit(solution)/shard_map/reduce_scatter | solution.py:46
  252.4 0.8 copy-start.9
  254.5 4.6 %copy-start.12 = (bf16[512,2048]{1,0:T(8,128)(2,1)S(1)}, bf16[512,2048]{1,0:T(8,128)(2,1)}, u32[]{:S(2)}) copy-start(bf16[512,2048]{1,0:T(8,128)(2,1)} %param.20) | copy-start | bytes 6291460
  262.7 44.8 %all-to-all-start.4 = ((f32[4,1,512]{2,1,0:T(1,128)}), f32[4,1,512]{2,1,0:T(1,128)S(1)}, u32[]{:S(2)}, u32[]{:S(2)}) async-start(f32[4,1,512]{2,1,0:T(1,128)} %broadcast_in_dim.20), calls=%async_computation.7 | async-start | bytes 16384 | tf_op jit(solution)/shard_map/all_to_all | solution.py:28
  266.0 61.6 %reduce-scatter.6.cloned.1.call-start = ((), (), s32[]{:S(2)}) async-start(), calls=%async_computation.10 | async-start | bytes 655360 | tf_op jit(solution)/shard_map/reduce_scatter | solution.py:46
  304.5 41.7 %reduce-scatter.8.cloned.1.call-start = ((), (), s32[]{:S(2)}) async-start(), calls=%async_computation.11 | async-start | bytes 196608 | tf_op jit(solution)/shard_map/reduce_scatter | solution.py:46
  308.8 0.8 copy-start.1
  309.6 17.9 %collective-permute-start = (f32[30,512]{1,0:T(8,128)S(1)}, f32[30,512]{1,0:T(8,128)S(1)}, u32[]{:S(2)}, u32[]{:S(2)}) collective-permute-start(f32[30,512]{1,0:T(8,128)S(1)} %slice.267), channel_id=1, source_target_pairs={{4,0},{8,4},{12,8},{16,12},{20,16},{24,20},{28,24},{32,28},{36,32}... | collective-permute-start | bytes 184328 | tf_op jit(solution)/shard_map/ppermute | solution.py:66
  315.5 12.1 %copy-start.6 = (bf16[256,512]{1,0:T(8,128)(2,1)S(1)}, bf16[256,512]{1,0:T(8,128)(2,1)}, u32[]{:S(2)}) copy-start(bf16[256,512]{1,0:T(8,128)(2,1)} %param.25) | copy-start | bytes 786436
Sparse Core Ops, SparseCore 0:
  64.1 47.6 all-gather.1
  252.5 51.9 reduce-scatter.3
  307.0 20.4 reduce-scatter.5
  330.4 15.7 reduce-scatter.7
where the time goes:
time: 354 us; the launch traced here: 353 us
  waiting for transfers between devices  123 us (35%)
  blocking collectives  96.7 us (27%)
  local copies, waits for them, and re-layouts  38.6 us (11%)
  matrix products  28.9 us (8%)
  other arithmetic  28.6 us (8%)
  starting transfers between devices  22.6 us (6%)
  between operations  14.1 us (4%)
    reduce_scatter x3, waiting for transfers between devices, sum_by_axis(): subtotal = lax.psum_scatter(subtotal, axis, scatter_dimension=0, tiled=True)  52.4 us
    all_gather x1, waiting for transfers between devices, per_device(): arrived = lax.all_gather(moved, 'tp', axis=2, tiled=True)  42.8 us
    all_to_all x1, blocking collectives, per_device(): lax.all_to_all(outgoing.reshape(group_size, capacity, local_cols), SP, sp...  41.2 us
    all_to_all x1, blocking collectives, sum_at_owner(): lax.all_to_all(tiles, axis, split_axis=0, concat_axis=0, tiled=True)  39.9 us
    all_to_all x1, waiting for transfers between devices, per_device(): lax.all_to_all(input_grad.reshape(group_size, capacity, local_cols), SP,...  28.1 us
    psum x1, blocking collectives, per_device(): lax.psum((jnp.sum(convolution_filter, axis=1), jnp.sum(convolution_filter...  15.6 us
    all_to_all x1, starting transfers between devices, per_device(): lax.all_to_all(input_grad.reshape(group_size, capacity, local_cols), SP,...  12.1 us
    convert_element_type x1, other arithmetic, per_device(): (d_glu * value_pre.astype(jnp.float32) * gate_sig * (1.0 - gate_sig)).ast...  11.4 us
  transfers between devices with their start and end apart: 8, of which 5 were waited for; matrix products, arithmetic and copies ran while one was open for 11% of the time, Pallas kernels for 0%

commit v1 on v0

--- a/solution.py
+++ b/solution.py
@@ -109,7 +109,10 @@
         concat_axis=0,
         tiled=True,
     )
-    arrived = lax.all_gather(moved, "tp", axis=2, tiled=True)
+    peers = lax.axis_size("tp")
+    blocks = jnp.stack([moved for _ in range(peers)])
+    blocks = lax.all_to_all(blocks, "tp", split_axis=0, concat_axis=0)
+    arrived = jnp.concatenate(blocks, axis=2)
     rows_cot = arrived.reshape(slot_rows, model_width)
     rows_in = expert_inputs[0]
     gate_weight = w_gate[0]

time: 354 us -> 344 us (0.972)
  waiting for transfers between devices: 123 us -> 112 us
    all_gather x1 -> x0, waiting for transfers between devices: 42.8 us -> none  [per_device(): arrived = lax.all_gather(moved, 'tp', axis=2, tiled=True)]
    all_to_all x0 -> x1, waiting for transfers between devices: none -> 31.6 us  [per_device(): blocks = lax.all_to_all(blocks, 'tp', split_axis=0, concat_axis=0)]
    all_to_all x0 -> x1, starting transfers between devices: none -> 4.82 us  [per_device(): blocks = lax.all_to_all(blocks, 'tp', split_axis=0, concat_axis=0)]
    unnamed x30 -> x39, local copies, waits for them, and re-layouts: 7.7 us -> 9.4 us
where the time goes in v1:
time: 344 us; the launch traced here: 342 us
  waiting for transfers between devices  112 us (33%)
  blocking collectives  95.8 us (28%)
  local copies, waits for them, and re-layouts  41 us (12%)
  other arithmetic  28.6 us (8%)
  matrix products  26.1 us (8%)
  starting transfers between devices  24.1 us (7%)
  between operations  14.1 us (4%)
    reduce_scatter x3, waiting for transfers between devices, sum_by_axis(): subtotal = lax.psum_scatter(subtotal, axis, scatter_dimension=0, tiled=True)  52.7 us
    all_to_all x1, blocking collectives, per_device(): lax.all_to_all(outgoing.reshape(group_size, capacity, local_cols), SP, sp...  41.1 us
    all_to_all x1, blocking collectives, sum_at_owner(): lax.all_to_all(tiles, axis, split_axis=0, concat_axis=0, tiled=True)  39.1 us
    all_to_all x1, waiting for transfers between devices, per_device(): blocks = lax.all_to_all(blocks, 'tp', split_axis=0, concat_axis=0)  31.6 us
    all_to_all x1, waiting for transfers between devices, per_device(): lax.all_to_all(input_grad.reshape(group_size, capacity, local_cols), SP,...  28.1 us
    psum x1, blocking collectives, per_device(): lax.psum((jnp.sum(convolution_filter, axis=1), jnp.sum(convolution_filter...  15.6 us
    convert_element_type x1, other arithmetic, per_device(): (d_glu * value_pre.astype(jnp.float32) * gate_sig * (1.0 - gate_sig)).ast...  11.4 us
    unnamed x39, local copies, waits for them, and re-layouts  9.4 us
  transfers between devices with their start and end apart: 8, of which 5 were waited for; matrix products, arithmetic and copies ran while one was open for 11% of the time, Pallas kernels for 0%

profile of v1, /device:TPU:1, one launch (start us, length us, event | category | flops | bytes accessed | tf_op | source)
XLA Modules:
  0.0 342.2 jit_solution(16583873522453403738)
XLA Ops:
  7.2 0.8 broadcast_multiply_fusion
  8.0 0.9 copy.62
  9.0 0.1 eq.25
  9.1 0.1 eq.29
  9.4 0.1 mul.445
  9.6 1.2 reduce-window.6
  10.8 0.2 slice_reduce_fusion
  11.0 2.2 broadcast_in_dim.15
  13.2 2.9 convert_element_type.80
  16.3 0.1 mul.447
  16.6 4.1 %scatter_custom_fusion = bf16[768,512]{1,0:T(8,128)(2,1)} fusion(s32[512]{0:T(512)S(1)} %bitcast.154, f32[512,512]{1,0:T(8,128)} %convert_element_type.80, f32[512]{0:T(512)S(1)} %mul.447, bf16[]{:T(256)} %constant.12.clone.1), kind=kCustom, calls=%fused_computation.199 | custom fusion | flops 524288 | bytes 1837058 | tf_op jit(solution)/shard_map/scatter | solution.py:103
  20.6 2.1 reshape.102
  22.7 41.1 %all_to_all.31 = bf16[64,12,512]{2,1,0:T(8,128)(2,1)S(1)} all-to-all(bf16[64,12,512]{2,1,0:T(8,128)(2,1)} %reshape.102), channel_id=1, replica_groups=mesh['sp_0'=8,'sp_1'=4,'sp_2'=2,'tp'=4] {'sp_0','sp_1','sp_2'}, dimensions={0} | all-to-all | bytes 1572864 | tf_op jit(solution)/shard_map/all_to_all | solution.py:105
  63.9 0.4 copy.66
  64.3 2.1 stack.2
  66.4 4.8 %all-to-all-start.1 = ((bf16[4,64,12,512]{3,1,2,0:T(8,128)(2,1)}), bf16[4,64,12,512]{3,1,2,0:T(8,128)(2,1)}, u32[]{:S(2)}, u32[]{:S(2)}) async-start(bf16[4,64,12,512]{3,1,2,0:T(8,128)(2,1)} %stack.2), calls=%async_computation.1 | async-start | bytes 6291456 | tf_op jit(solution)/shard_map/all_to_all | solution.py:114
  71.2 3.2 fusion.4
  74.4 1.9 fusion.6
  76.3 31.6 %all-to-all-done.1 = bf16[4,64,12,512]{3,1,2,0:T(8,128)(2,1)} async-done(((bf16[4,64,12,512]{3,1,2,0:T(8,128)(2,1)}), bf16[4,64,12,512]{3,1,2,0:T(8,128)(2,1)}, u32[]{:S(2)}, u32[]{:S(2)}) %all-to-all-start.1) | async-done | bytes 3145760 | tf_op jit(solution)/shard_map/all_to_all | solution.py:114
  107.9 4.3 %copy.67 = bf16[64,12,4,512]{3,2,1,0:T(4,128)(2,1)S(1)} copy(bf16[64,12,4,512]{3,0,1,2:T(8,128)(2,1)} %bitcast.5) | data formatting | bytes 6291456 | tf_op jit(solution)/shard_map/reshape | solution.py:115
  112.2 1.0 copy.78
  113.4 0.2 copy-done.15
  113.7 0.2 copy-done.16
  113.9 1.4 select_convert_fusion
  115.4 0.2 copy-done.6
  115.6 1.0 fusion.27
  116.7 0.2 copy-done.8
  116.9 1.0 add_convert_fusion
  117.9 0.2 copy.81
  118.1 39.1 %all_to_all.32 = bf16[4,768,512]{2,1,0:T(8,128)(2,1)} all-to-all(bf16[4,768,512]{2,1,0:T(8,128)(2,1)S(1)} %bitcast.118), channel_id=1, replica_groups=mesh['sp_0'=8,'sp_1'=4,'sp_2'=2,'tp'=4] {'tp'}, dimensions={0} | all-to-all | bytes 6291456 | tf_op jit(solution)/shard_map/all_to_all | solution.py:22
  157.2 3.5 %reduce_sum.81 = bf16[768,512]{1,0:T(8,128)(2,1)} reduce(bf16[4,768,512]{2,1,0:T(8,128)(2,1)} %all_to_all.32, bf16[]{:T(256)} %constant.12.clone.1), dimensions={0}, to_apply=%region_8.9 | reduce | flops 1179648 | bytes 3932162 | tf_op jit(solution)/shard_map/reduce_sum | solution.py:23
  160.7 2.1 reshape.105
  162.8 9.1 %all-to-all-start.3 = ((bf16[64,12,512]{2,1,0:T(8,128)(2,1)}), bf16[64,12,512]{2,1,0:T(8,128)(2,1)}, u32[]{:S(2)}, u32[]{:S(2)}) async-start(bf16[64,12,512]{2,1,0:T(8,128)(2,1)} %reshape.105), calls=%async_computation.3 | async-start | bytes 2097152 | tf_op jit(solution)/shard_map/all_to_all | solution.py:142
  171.9 28.1 %all-to-all-done.3 = bf16[64,12,512]{2,1,0:T(8,128)(2,1)} async-done(((bf16[64,12,512]{2,1,0:T(8,128)(2,1)}), bf16[64,12,512]{2,1,0:T(8,128)(2,1)}, u32[]{:S(2)}, u32[]{:S(2)}) %all-to-all-start.3) | async-done | bytes 786464 | tf_op jit(solution)/shard_map/all_to_all | solution.py:142
  200.0 2.1 reshape.106
  202.0 3.9 %gather_fusion = bf16[512,512]{1,0:T(8,128)(2,1)} fusion(bf16[768,512]{1,0:T(8,128)(2,1)} %reshape.106, s32[1024]{0:T(1024)S(1)} %pad_clamp_fusion), kind=kCustom, calls=%fused_computation | custom fusion | bytes 1050624 | tf_op jit(solution)/shard_map/gather | solution.py:149
  205.9 2.7 reshape.108
  208.6 3.3 reduce_sum.82
  211.9 1.9 add_convert_fusion.1
  213.7 1.8 copy.69
  215.5 2.0 broadcast_in_dim.19
  217.5 4.2 %all-to-all-start.4 = ((bf16[4,256,512]{1,2,0:T(8,128)(2,1)}), bf16[4,256,512]{1,2,0:T(8,128)(2,1)}, u32[]{:S(2)}, u32[]{:S(2)}) async-start(bf16[4,256,512]{1,2,0:T(8,128)(2,1)} %broadcast_in_dim.19), calls=%async_computation.4 | async-start | bytes 2097152 | tf_op jit(solution)/shard_map/all_to_all | solution.py:28
  221.8 0.2 convert_reduce_fusion
  222.0 15.6 %all-reduce = (f32[256]{0:T(256)S(1)}, f32[256]{0:T(256)S(1)}) all-reduce(f32[256]{0:T(256)S(1)} %get-tuple-element.45, f32[256]{0:T(256)S(1)} %get-tuple-element.44), channel_id=1, replica_groups=mesh['sp_0'=8,'sp_1'=4,'sp_2'=2,'tp'=4] {'tp'}, use_global_device_ids=true, to_apply=%region_7.8 | all-reduce | flops 512 | bytes 4096 | tf_op jit(solution)/shard_map/psum | solution.py:155
  237.6 4.1 %fusion.142 = f32[512,2048]{1,0:T(8,128)} fusion(bf16[256,2048]{0,1:T(8,128)(2,1)} %bitcast.15, bf16[256,512]{1,0:T(8,128)(2,1)S(1)} %copy-done.3, f32[512]{0:T(512)S(1)} %copy-done.12, f32[256]{0:T(256)S(1)} %get-tuple-element.86, f32[256]{0:T(256)S(1)} %get-tuple-element.85), kind=kOutput, calls=%fused_computation.212 | convolution fusion | flops 538050560 | bytes 5509120 | tf_op jit(solution)/shard_map/dot_general | solution.py:170
  241.7 0.8 copy-done.10
  242.5 0.6 fusion.160
  243.2 0.7 fusion.159
  243.8 4.6 %fusion.14 = bf16[1,256,2048]{2,1,0:T(8,128)(2,1)} fusion(bf16[768,2048]{1,0:T(8,128)(2,1)} %bitcast.121, f32[768,256]{1,0:T(8,128)} %fusion.6, f32[768,256]{1,0:T(8,128)} %fusion.4), kind=kOutput, calls=%fused_computation.44 | convolution fusion | flops 807796736 | bytes 5767168 | tf_op jit(solution)/shard_map/dot_general | solution.py:127
  248.5 3.0 fusion.157
  251.4 0.6 broadcast_in_dim.20
  252.0 3.2 all-to-all-start.5
  255.4 38.5 %reduce-scatter.4.cloned.1.call-done = f32[64,2048]{1,0:T(8,128)} async-done(((f32[512,2048]{1,0:T(8,128)}), f32[64,2048]{1,0:T(8,128)}) %reduce-scatter.4.cloned.1.call-update) | async-done | bytes 524304 | tf_op jit(solution)/shard_map/reduce_scatter | solution.py:46
  293.9 3.0 fusion.18
  296.9 1.2 fusion.132
  298.1 0.8 copy-done.2
  299.0 2.6 collective-permute-start
  301.6 3.0 fusion.15
  304.6 2.3 copy.71
  306.9 2.3 copy.72
  309.2 7.7 %reduce-scatter.6.cloned.1.call-done = f32[16,2048]{1,0:T(8,128)} async-done(((f32[64,2048]{1,0:T(8,128)}), f32[16,2048]{1,0:T(8,128)}) %reduce-scatter.6.cloned.1.call-update) | async-done | bytes 131088 | tf_op jit(solution)/shard_map/reduce_scatter | solution.py:46
  316.9 11.4 %multiply_convert_fusion.3 = (bf16[256,512]{1,0:T(8,128)(2,1)}, f32[256,512]{1,0:T(8,128)S(1)}) fusion(bf16[256,512]{1,0:T(8,128)(2,1)} %param.24, bf16[256,512]{1,0:T(8,128)(2,1)S(1)} %copy-done.7, f32[256,512]{1,0:T(8,128)} %copy-done.2, f32[512]{0:T(512)} %bitcast.132, f32[30,512]{1,0:T(8,128)S(1)} %collective-permute-done, f32[512]{0:T(512)} %bitcast.133, ...), kind=kLoop, calls=%fused_computation.202 | loop fusion | flops 13238272 | bytes 1959936 | tf_op jit(solution)/shard_map/convert_element_type | solution.py:203
  328.3 0.9 multiply_convert_fusion.4
  329.2 6.5 %reduce-scatter.8.cloned.1.call-done = f32[8,2048]{1,0:T(8,128)} async-done(((f32[16,2048]{1,0:T(8,128)}), f32[8,2048]{1,0:T(8,128)}) %reduce-scatter.8.cloned.1.call-update) | async-done | bytes 65552 | tf_op jit(solution)/shard_map/reduce_scatter | solution.py:46
  (50 shorter events, 0.9 us)
Async XLA Ops:
  7.2 64.0 %copy-start = (bf16[1,768,2048]{2,1,0:T(8,128)(2,1)S(1)}, bf16[1,768,2048]{2,1,0:T(8,128)(2,1)}, u32[]{:S(2)}) copy-start(bf16[1,768,2048]{2,1,0:T(8,128)(2,1)} %param.16) | copy-start | bytes 9437188
  7.2 9.0 %copy-start.11 = (f32[256,2]{0,1:T(2,128)S(1)}, f32[256,2]{0,1:T(2,128)}, u32[]{:S(2)}) copy-start(f32[256,2]{0,1:T(2,128)} %param.15) | copy-start | bytes 6148
  66.4 41.5 %all-to-all-start.1 = ((bf16[4,64,12,512]{3,1,2,0:T(8,128)(2,1)}), bf16[4,64,12,512]{3,1,2,0:T(8,128)(2,1)}, u32[]{:S(2)}, u32[]{:S(2)}) async-start(bf16[4,64,12,512]{3,1,2,0:T(8,128)(2,1)} %stack.2), calls=%async_computation.1 | async-start | bytes 6291456 | tf_op jit(solution)/shard_map/all_to_all | solution.py:114
  71.2 3.2 copy-start.5
  112.2 1.2 copy-start.14
  112.2 1.4 copy-start.15
  112.2 1.7 copy-start.16
  113.3 2.0 copy-start.1
  113.9 1.7 copy-start.6
  115.4 1.3 copy-start.4
  115.4 1.3 copy-start.9
  115.6 1.2 copy-start.8
  162.8 37.1 %all-to-all-start.3 = ((bf16[64,12,512]{2,1,0:T(8,128)(2,1)}), bf16[64,12,512]{2,1,0:T(8,128)(2,1)}, u32[]{:S(2)}, u32[]{:S(2)}) async-start(bf16[64,12,512]{2,1,0:T(8,128)(2,1)} %reshape.105), calls=%async_computation.3 | async-start | bytes 2097152 | tf_op jit(solution)/shard_map/all_to_all | solution.py:142
  208.6 13.3 %copy-start.3 = (bf16[256,512]{1,0:T(8,128)(2,1)S(1)}, bf16[256,512]{1,0:T(8,128)(2,1)}, u32[]{:S(2)}) copy-start(bf16[256,512]{1,0:T(8,128)(2,1)} %param.21) | copy-start | bytes 786436
  208.6 29.0 %copy-start.12 = (f32[512]{0:T(512)S(1)}, f32[512]{0:T(512)}, u32[]{:S(2)}) copy-start(f32[512]{0:T(512)} %param.22) | copy-start | bytes 6148
  217.5 20.1 %all-to-all-start.4 = ((bf16[4,256,512]{1,2,0:T(8,128)(2,1)}), bf16[4,256,512]{1,2,0:T(8,128)(2,1)}, u32[]{:S(2)}, u32[]{:S(2)}) async-start(bf16[4,256,512]{1,2,0:T(8,128)(2,1)} %broadcast_in_dim.19), calls=%async_computation.4 | async-start | bytes 2097152 | tf_op jit(solution)/shard_map/all_to_all | solution.py:28
  221.8 72.0 %reduce-scatter.4.cloned.1.call-start = ((), (), s32[]{:S(2)}) async-start(), calls=%async_computation.9 | async-start | bytes 4718592 | tf_op jit(solution)/shard_map/reduce_scatter | solution.py:46
  241.7 0.8 copy-start.10
  243.8 4.6 %copy-start.13 = (bf16[512,2048]{1,0:T(8,128)(2,1)S(1)}, bf16[512,2048]{1,0:T(8,128)(2,1)}, u32[]{:S(2)}) copy-start(bf16[512,2048]{1,0:T(8,128)(2,1)} %param.20) | copy-start | bytes 6291460
  252.0 44.8 %all-to-all-start.5 = ((f32[4,1,512]{2,1,0:T(1,128)}), f32[4,1,512]{2,1,0:T(1,128)S(1)}, u32[]{:S(2)}, u32[]{:S(2)}) async-start(f32[4,1,512]{2,1,0:T(1,128)} %broadcast_in_dim.20), calls=%async_computation.8 | async-start | bytes 16384 | tf_op jit(solution)/shard_map/all_to_all | solution.py:28
  255.3 61.6 %reduce-scatter.6.cloned.1.call-start = ((), (), s32[]{:S(2)}) async-start(), calls=%async_computation.10 | async-start | bytes 655360 | tf_op jit(solution)/shard_map/reduce_scatter | solution.py:46
  293.8 41.9 %reduce-scatter.8.cloned.1.call-start = ((), (), s32[]{:S(2)}) async-start(), calls=%async_computation.11 | async-start | bytes 196608 | tf_op jit(solution)/shard_map/reduce_scatter | solution.py:46
  298.1 0.8 copy-start.2
  299.0 18.0 %collective-permute-start = (f32[30,512]{1,0:T(8,128)S(1)}, f32[30,512]{1,0:T(8,128)S(1)}, u32[]{:S(2)}, u32[]{:S(2)}) collective-permute-start(f32[30,512]{1,0:T(8,128)S(1)} %slice.267), channel_id=1, source_target_pairs={{4,0},{8,4},{12,8},{16,12},{20,16},{24,20},{28,24},{32,28},{36,32}... | collective-permute-start | bytes 184328 | tf_op jit(solution)/shard_map/ppermute | solution.py:66
  304.6 12.3 %copy-start.7 = (bf16[256,512]{1,0:T(8,128)(2,1)S(1)}, bf16[256,512]{1,0:T(8,128)(2,1)}, u32[]{:S(2)}) copy-start(bf16[256,512]{1,0:T(8,128)(2,1)} %param.25) | copy-start | bytes 786436
Sparse Core Ops, SparseCore 0:
  241.8 51.9 reduce-scatter.3
  296.3 20.5 reduce-scatter.5
  319.9 15.6 reduce-scatter.7
